TPU v7x, 32 devices: a whole 2x2x4 slice. The times are simulated.
32 devices in a mesh: sp: 8 (over z, y), tp: 4 (over x, core).
Axes of the slice: x: 2, y: 2, z: 4, core: 2. Of those that a mesh axis runs over, the one named last changes fastest.
Arguments:
- queries: bfloat16 [8192, 8, 128], P('sp', 'tp'), may hold values from -160 to 160
- keys_values: bfloat16 [8192, 8, 128], P('sp', 'tp'), may hold values from -5 to 5
- sink_logits: float32 [8, 2], P('tp'), may hold values from 2 to 7
- doc_ids: int32 [8192], replicated, may hold values from 0 to 5, never falling along the last dimension, each value on 1 to 4096 neighbouring positions
- residual: bfloat16 [8192, 2048], P('sp'), may hold values from -6 to 6
- out_weight: bfloat16 [1024, 2048], P('tp'), may hold values from -1.5 to 1.5
- ffn_gain: float32 [2048], replicated, may hold values from 0.1 to 1.9
- gate_weight: bfloat16 [2048, 5120], P('sp', 'tp'), may hold values from -0.125 to 0.125
- value_weight: bfloat16 [2048, 5120], P('sp', 'tp'), may hold values from -0.125 to 0.125
- conv_taps: float32 [3, 5120], P(None, 'tp'), may hold values from -4 to 4
- down_weight: bfloat16 [2048, 5120], P('sp', 'tp'), may hold values from -0.078125 to 0.078125
Outputs:
- layer_out: bfloat16 [8192, 2048], P(('sp', 'tp'))
Inputs may be any that keep to these rules, and one draw needn't show every extreme that they name: `doc_ids`: document numbers never fall along the sequence; a document spans at most 4096 positions.
All inputs are finite; a program needn't handle non-finite values.
Results may differ from a plain program's by a relative error of at most 0.02.
Values may be sent and summed in bfloat16 or wider, within the bound.
A program may use at most 128 MiB of HBM per device.

v0:
```python
import jax
import jax.numpy as jnp
from jax import lax
from jax.sharding import PartitionSpec as P

HEAD_DIM = 64
WINDOW = 128
norm_epsilon = 1e-06
masked_score = -1e30
contract_last = (((1,), (1,)), ((), ()))


def extended_2(cells, sides, width):
    for axis, dim in sides:
        count = lax.axis_size(axis)
        ends = count - 1
        head = lax.slice_in_dim(cells, 0, width, axis=dim)
        tail = lax.slice_in_dim(cells, cells.shape[dim] - width, cells.shape[dim], axis=dim)
        cells = jnp.concatenate(
            [
                lax.ppermute(tail, axis, [(i, (i + 1) % count) for i in range(ends)]),
                cells,
                lax.ppermute(head, axis, [((i + 1) % count, i) for i in range(ends)]),
            ],
            axis=dim,
        )
    return cells


def band_blocks(padded, block_count, window_rows):
    row_block = padded.reshape((block_count + 2, window_rows) + padded.shape[1:])
    return jnp.concatenate([row_block[:-2], row_block[1:-1], row_block[2:]], axis=1)


def normalize(stream, gain):
    stream_f = stream.astype(jnp.float32)
    scale = lax.rsqrt(jnp.mean(stream_f * stream_f, axis=-1, keepdims=True) + norm_epsilon)
    return (stream_f * scale * gain).astype(jnp.bfloat16)


def attend(queries, keys_values, sink_logits, doc_ids, offset):
    local_rows = queries.shape[0]
    kv_local = queries.shape[1]
    head_dim = HEAD_DIM
    group_size = queries.shape[2] // head_dim
    window_rows = WINDOW
    block_count = local_rows // window_rows
    padded = extended_2(keys_values, (("sp", 0),), window_rows)
    blocks = band_blocks(padded, block_count, window_rows)
    key_blocks = blocks[..., :head_dim]
    value_blocks = blocks[..., head_dim:]
    query_blocks = queries.reshape(block_count, window_rows, kv_local, group_size, head_dim)
    scores = jnp.einsum(
        "nqkgd,nskd->nkgqs", query_blocks, key_blocks, preferred_element_type=jnp.float32
    ) * head_dim ** (-0.5)
    padded_docs = jnp.pad(doc_ids, window_rows, constant_values=-1)
    near_docs = lax.dynamic_slice_in_dim(padded_docs, offset, local_rows + 2 * window_rows)
    key_docs = band_blocks(near_docs, block_count, window_rows)
    query_docs = near_docs[window_rows : window_rows + local_rows].reshape(block_count, window_rows)
    distance = jnp.arange(window_rows)[:, None] + window_rows - jnp.arange(3 * window_rows)[None, :]
    allowed = (jnp.abs(distance) <= WINDOW)[None] & (query_docs[:, :, None] == key_docs[:, None, :])
    scores = jnp.where(allowed[:, None, None], scores, masked_score)
    sink_part = sink_logits[None, :, :, None, None]
    top_score = jnp.maximum(jnp.max(scores, axis=-1, keepdims=True), sink_part)
    exp_scores = jnp.exp(scores - top_score)
    denominator = jnp.sum(exp_scores, axis=-1, keepdims=True) + jnp.exp(sink_part - top_score)
    probs = (exp_scores / denominator).astype(jnp.bfloat16)
    result = jnp.einsum(
        "nkgqs,nskd->nqkgd", probs, value_blocks, preferred_element_type=jnp.float32
    )
    return result.reshape(local_rows, kv_local * group_size * head_dim).astype(jnp.bfloat16)


def on_device(
    queries,
    keys_values,
    sink_logits,
    doc_ids,
    residual,
    out_weight,
    ffn_gain,
    gate_weight,
    value_weight,
    conv_taps,
    down_weight,
):
    local_rows = queries.shape[0]
    offset = lax.axis_index("sp") * local_rows
    tp_count = lax.axis_size("tp")
    part_rows = local_rows // tp_count
    row_start = lax.axis_index("tp") * part_rows
    gate_whole, value_whole, down_whole = (
        lax.all_gather(gate_weight, "sp", axis=0, tiled=True),
        lax.all_gather(value_weight, "sp", axis=0, tiled=True),
        lax.all_gather(down_weight, "sp", axis=0, tiled=True),
    )
    attended = attend(queries, keys_values, sink_logits, doc_ids, offset)
    partial_value = jnp.dot(attended, out_weight, preferred_element_type=jnp.float32)
    projected = lax.psum(partial_value.astype(jnp.bfloat16), "tp").astype(jnp.float32)
    stream = (residual.astype(jnp.float32) + projected).astype(jnp.bfloat16)
    normed = normalize(stream, ffn_gain)
    stream_rows = lax.dynamic_slice_in_dim(stream, row_start, part_rows, 0)
    gate_pre = jnp.dot(normed, gate_whole, preferred_element_type=jnp.float32)
    value_pre = jnp.dot(normed, value_whole, preferred_element_type=jnp.float32)
    gate_stored = gate_pre.astype(jnp.bfloat16)
    extended = extended_2(gate_stored, (("sp", 0),), 1).astype(jnp.float32)
    padded_docs = jnp.pad(doc_ids, 1, constant_values=-1)
    near_docs = lax.dynamic_slice_in_dim(padded_docs, offset, local_rows + 2)
    prev_same = (near_docs[1:-1] == near_docs[:-2]).astype(jnp.float32)[:, None]
    next_same = (near_docs[1:-1] == near_docs[2:]).astype(jnp.float32)[:, None]
    conved = (
        conv_taps[0] * extended[:-2] * prev_same
        + conv_taps[1] * extended[1:-1]
        + conv_taps[2] * extended[2:] * next_same
    )
    hidden = (jax.nn.gelu(conved, approximate=True) * value_pre).astype(jnp.bfloat16)
    lowered = lax.psum_scatter(
        lax.dot_general(
            hidden, down_whole, contract_last, preferred_element_type=jnp.float32
        ).astype(jnp.bfloat16),
        "tp",
        scatter_dimension=0,
        tiled=True,
    ).astype(jnp.float32)
    return (stream_rows.astype(jnp.float32) + lowered).astype(jnp.bfloat16)


def solution(mesh):
    in_specs = (
        P("sp", "tp", None),
        P("sp", "tp", None),
        P("tp", None),
        P(),
        P("sp", None),
        P("tp", None),
        P(),
        P("sp", "tp"),
        P("sp", "tp"),
        P(None, "tp"),
        P("sp", "tp"),
    )
    out_specs = P(("sp", "tp"), None)
    return jax.shard_map(
        on_device, mesh=mesh, in_specs=in_specs, out_specs=out_specs, check_vma=False
    )
```

profile of v0, /device:TPU:0, one launch (start us, length us, event | category | flops | bytes accessed | tf_op | source)
XLA Modules:
  0.0 373.3 jit_solution(15646280819645604768)
XLA Ops:
  7.4 1.2 copy.14
  8.6 4.9 %collective-permute-start = (bf16[128,2,128]{2,0,1:T(8,128)(2,1)S(1)}, bf16[128,2,128]{2,0,1:T(8,128)(2,1)S(1)}, u32[]{:S(2)}, u32[]{:S(2)}) collective-permute-start(bf16[128,2,128]{2,0,1:T(8,128)(2,1)S(1)} %get-tuple-element.14), channel_id=1, source_target_pairs={{0,4},{4,8},{8,12},{12,16},{16,20},{20,24},{24,28},{1,5},{5,9},{9,... | collective-permute-start | bytes 196616 | tf_op jit(solution)/shard_map/ppermute | solution.py:21
  13.5 1.3 collective-permute-start.1
  14.9 0.9 fusion.31
  16.4 1.3 copy.20
  17.7 3.7 reshape.100
  22.0 1.0 pad_maximum_fusion.2
  23.9 2.5 fusion.17
  26.4 1.6 fusion.3
  28.1 1.8 fusion.20
  30.2 3.2 convolution_convert_fusion.2
  35.6 86.5 %all-reduce.4.cloned.1.call-done = bf16[1024,2048]{1,0:T(8,128)(2,1)} async-done(((bf16[1024,2048]{1,0:T(8,128)(2,1)}), bf16[1024,2048]{1,0:T(8,128)(2,1)}) %all-reduce.4.cloned.1.call-update) | async-done | bytes 4194320 | tf_op jit(solution)/shard_map/psum | solution.py:99
  122.1 7.4 %fusion = (f32[1024]{0:T(1024)S(1)}, bf16[1024,2048]{1,0:T(8,128)(2,1)}) fusion(bf16[1024,2048]{1,0:T(8,128)(2,1)} %all-reduce.4.cloned.1.call-done, bf16[1024,2048]{1,0:T(8,128)(2,1)} %param.15), kind=kLoop, calls=%fused_computation.2 | loop fusion | flops 14679040 | bytes 12587008 | tf_op jit(solution)/shard_map/reduce_sum | solution.py:37
  129.5 9.3 %convolution_convert_fusion = bf16[1024,1280]{1,0:T(8,128)(2,1)S(1)} fusion(bf16[2048,1280]{1,0:T(8,128)(2,1)} %all-gather.4.cloned.1.call-done, bf16[1024,2048]{1,0:T(8,128)(2,1)} %get-tuple-element.9, f32[2048]{0:T(1024)S(1)} %copy-done.7, f32[1024]{0:T(1024)S(1)} %add_rsqrt_fusion), kind=kOutput, calls=%fused_computation.28 | convolution fusion | flops 5378408448 | bytes 12070912 | tf_op jit(solution)/shard_map/dot_general | solution.py:103
  138.8 3.3 collective-permute-start.2
  142.2 1.3 collective-permute-start.3
  143.6 4.1 %collective-permute-done.3 = bf16[1,1280]{1,0:T(2,128)(2,1)S(1)} collective-permute-done((bf16[1,1280]{1,0:T(2,128)(2,1)S(1)}, bf16[1,1280]{1,0:T(2,128)(2,1)S(1)}, u32[]{:S(2)}, u32[]{:S(2)}) %collective-permute-start.3) | collective-permute-done | bytes 2592 | tf_op jit(solution)/shard_map/ppermute | solution.py:23
  147.7 13.4 %concatenate.20 = bf16[1026,1280]{1,0:T(8,128)(2,1)S(1)} concatenate(bf16[1,1280]{1,0:T(2,128)(2,1)S(1)} %collective-permute-done.2, bf16[1024,1280]{1,0:T(8,128)(2,1)} %copy-done.2, bf16[1,1280]{1,0:T(2,128)(2,1)S(1)} %collective-permute-done.3), dimensions={0} | concatenate | bytes 5253120 | tf_op jit(solution)/shard_map/concatenate | solution.py:19
  161.0 2.7 convert_element_type.69
  163.8 47.1 %all-gather.6.cloned.1.call-done = bf16[2048,1280]{1,0:T(8,128)(2,1)} async-done(((bf16[256,1280]{1,0:T(8,128)(2,1)}), bf16[2048,1280]{1,0:T(8,128)(2,1)}) %all-gather.6.cloned.1.call-update) | async-done | bytes 5242896 | tf_op jit(solution)/shard_map/all_gather | solution.py:94
  210.9 86.0 %all-gather.8.cloned.1.call-done = bf16[2048,1280]{1,0:T(8,128)(2,1)} async-done(((bf16[256,1280]{1,0:T(8,128)(2,1)}), bf16[2048,1280]{1,0:T(8,128)(2,1)}) %all-gather.8.cloned.1.call-update) | async-done | bytes 5242896 | tf_op jit(solution)/shard_map/all_gather | solution.py:95
  296.8 22.9 %convolution_convert_fusion.1 = bf16[1024,2048]{1,0:T(8,128)(2,1)} fusion(bf16[2048,1280]{1,0:T(8,128)(2,1)} %all-gather.8.cloned.1.call-done, f32[1026,1280]{1,0:T(8,128)} %convert_element_type.69, bf16[2048,1280]{1,0:T(8,128)(2,1)} %all-gather.6.cloned.1.call-done, f32[1024]{0:T(1024)S(1)} %get-tuple-element.17, f32[1280]{0:T(1024)S(1)} %get-tuple-element.6, ...), kind=kOutput, calls=%fused_computation.29 | convolution fusion | flops 10770186240 | bytes 34638848 | tf_op jit(solution)/shard_map/dot_general | solution.py:118
  319.8 43.0 %reduce-scatter.2.cloned.1.call-done = bf16[256,2048]{1,0:T(8,128)(2,1)} async-done(((bf16[1024,2048]{1,0:T(8,128)(2,1)}), bf16[256,2048]{1,0:T(8,128)(2,1)}) %reduce-scatter.2.cloned.1.call-update) | async-done | bytes 1048592 | tf_op jit(solution)/shard_map/reduce_scatter | solution.py:117
  362.8 2.9 add_convert_fusion.1
  (45 shorter events, 4.7 us)
Async XLA Ops:
  7.4 22.8 %copy-start = (bf16[256,2048]{1,0:T(8,128)(2,1)S(1)}, bf16[256,2048]{1,0:T(8,128)(2,1)}, u32[]{:S(2)}) copy-start(bf16[256,2048]{1,0:T(8,128)(2,1)} %param.16) | copy-start | bytes 3145732
  7.4 114.7 %all-reduce.4.cloned.1.call-start = ((), (), s32[]{:S(2)}) async-start(), calls=%async_computation.1 | async-start | bytes 8388608 | tf_op jit(solution)/shard_map/psum | solution.py:99
  8.6 12.8 %collective-permute-start = (bf16[128,2,128]{2,0,1:T(8,128)(2,1)S(1)}, bf16[128,2,128]{2,0,1:T(8,128)(2,1)S(1)}, u32[]{:S(2)}, u32[]{:S(2)}) collective-permute-start(bf16[128,2,128]{2,0,1:T(8,128)(2,1)S(1)} %get-tuple-element.14), channel_id=1, source_target_pairs={{0,4},{4,8},{8,12},{12,16},{16,20},{20,24},{24,28},{1,5},{5,9},{9,... | collective-permute-start | bytes 196616 | tf_op jit(solution)/shard_map/ppermute | solution.py:21
  13.5 8.5 %collective-permute-start.1 = (bf16[128,2,128]{2,0,1:T(8,128)(2,1)S(1)}, bf16[128,2,128]{2,0,1:T(8,128)(2,1)}, u32[]{:S(2)}, u32[]{:S(2)}) collective-permute-start(bf16[128,2,128]{2,0,1:T(8,128)(2,1)S(1)} %get-tuple-element.15), channel_id=1, source_target_pairs={{4,0},{8,4},{12,8},{16,12},{20,16},{24,20},{28,24},{5,1},{9,5},{13... | collective-permute-start | bytes 196616 | tf_op jit(solution)/shard_map/ppermute | solution.py:23
  21.4 0.6 copy-start.4
  23.6 2.8 copy-start.6
  30.2 5.3 %copy-start.5 = (f32[3,1280]{1,0:T(4,128)S(1)}, f32[3,1280]{1,0:T(4,128)}, u32[]{:S(2)}) copy-start(f32[3,1280]{1,0:T(4,128)} %param.20) | copy-start | bytes 46084
  33.5 96.0 %all-gather.4.cloned.1.call-start = ((), (), s32[]{:S(2)}) async-start(), calls=%async_computation.2 | async-start | bytes 5898240 | tf_op jit(solution)/shard_map/all_gather | solution.py:93
  34.1 176.8 %all-gather.6.cloned.1.call-start = ((), (), s32[]{:S(2)}) async-start(), calls=%async_computation.3 | async-start | bytes 5898240 | tf_op jit(solution)/shard_map/all_gather | solution.py:94
  34.7 262.2 %all-gather.8.cloned.1.call-start = ((), (), s32[]{:S(2)}) async-start(), calls=%async_computation.4 | async-start | bytes 5898240 | tf_op jit(solution)/shard_map/all_gather | solution.py:95
  35.3 327.5 %reduce-scatter.2.cloned.1.call-start = ((), (), s32[]{:S(2)}) async-start(), calls=%async_computation.5 | async-start | bytes 5242880 | tf_op jit(solution)/shard_map/reduce_scatter | solution.py:117
  35.5 93.9 %copy-start.7 = (f32[2048]{0:T(1024)S(1)}, f32[2048]{0:T(1024)}, u32[]{:S(2)}) copy-start(f32[2048]{0:T(1024)} %param.17) | copy-start | bytes 24580
  129.5 14.0 %copy-start.3 = (s32[8192]{0:T(1024)S(1)}, s32[8192]{0:T(1024)}, u32[]{:S(2)}) copy-start(s32[8192]{0:T(1024)} %param.14) | copy-start | bytes 98308
  138.8 4.8 %copy-start.2 = (bf16[1024,1280]{1,0:T(8,128)(2,1)}, bf16[1024,1280]{1,0:T(8,128)(2,1)S(1)}, u32[]{:S(2)}) copy-start(bf16[1024,1280]{1,0:T(8,128)(2,1)S(1)} %convolution_convert_fusion) | copy-start | bytes 7864324
  138.8 4.7 %collective-permute-start.2 = (bf16[1,1280]{1,0:T(2,128)(2,1)S(1)}, bf16[1,1280]{1,0:T(2,128)(2,1)S(1)}, u32[]{:S(2)}, u32[]{:S(2)}) collective-permute-start(bf16[1,1280]{1,0:T(2,128)(2,1)S(1)} %get-tuple-element.11), channel_id=1, source_target_pairs={{0,4},{4,8},{8,12},{12,16},{16,20},{20,24},{24,28},{1,5},{5,9},{9,... | collective-permute-start | bytes 7688 | tf_op jit(solution)/shard_map/ppermute | solution.py:21
  142.2 5.5 %collective-permute-start.3 = (bf16[1,1280]{1,0:T(2,128)(2,1)S(1)}, bf16[1,1280]{1,0:T(2,128)(2,1)S(1)}, u32[]{:S(2)}, u32[]{:S(2)}) collective-permute-start(bf16[1,1280]{1,0:T(2,128)(2,1)S(1)} %get-tuple-element.10), channel_id=1, source_target_pairs={{4,0},{8,4},{12,8},{16,12},{20,16},{24,20},{28,24},{5,1},{9,5},{13... | collective-permute-start | bytes 7688 | tf_op jit(solution)/shard_map/ppermute | solution.py:23
  296.8 68.8 %copy-start.1 = (bf16[256,2048]{1,0:T(8,128)(2,1)S(1)}, bf16[256,2048]{1,0:T(8,128)(2,1)}, u32[]{:S(2)}) copy-start(bf16[256,2048]{1,0:T(8,128)(2,1)} %param.16) | copy-start | bytes 3145732
Sparse Core Ops, SparseCore 0:
  33.6 88.4 all-reduce.3
  319.9 42.8 reduce-scatter.1
Sparse Core Ops, SparseCore 1:
  36.2 88.5 all-gather.3
  126.8 84.0 all-gather.5
  212.9 83.9 all-gather.7
where the time goes:
time: 374 us; the launch traced here: 373 us
  waiting for transfers between devices  268 us (72%)
  matrix products  39.7 us (11%)
  local copies, waits for them, and re-layouts  22.1 us (6%)
  other arithmetic  16.8 us (4%)
  between operations  15.3 us (4%)
  starting transfers between devices  11.1 us (3%)
    psum x1, waiting for transfers between devices, on_device(): lax.psum(partial_value.astype(jnp.bfloat16), 'tp').astype(jnp.float32)  86.5 us
    all_gather x1, waiting for transfers between devices, on_device(): lax.all_gather(down_weight, 'sp', axis=0, tiled=True)  86 us
    all_gather x1, waiting for transfers between devices, on_device(): lax.all_gather(value_weight, 'sp', axis=0, tiled=True)  47.1 us
    reduce_scatter x1, waiting for transfers between devices, on_device(): lax.psum_scatter(lax.dot_general(hidden, down_whole, contract_last, prefe...  43 us
    dot_general x1, matrix products, on_device(): lax.dot_general(hidden, down_whole, contract_last, preferred_element_type...  22.9 us
    concatenate x1, local copies, waits for them, and re-layouts, extended_2(): jnp.concatenate([lax.ppermute(tail, axis, [(i, (i + 1) % count) for i in...  13.4 us
    dot_general x1, matrix products, on_device(): gate_pre = jnp.dot(normed, gate_whole, preferred_element_type=jnp.float32)  9.3 us
    ppermute x2, starting transfers between devices, extended_2(): lax.ppermute(tail, axis, [(i, (i + 1) % count) for i in range(ends)])  8.22 us
  transfers between devices with their start and end apart: 9, of which 5 were waited for; matrix products, arithmetic and copies ran while one was open for 11% of the time, Pallas kernels for 0%

commit v1 on v0

--- a/solution.py
+++ b/solution.py
@@ -91,7 +91,9 @@
     row_start = lax.axis_index("tp") * part_rows
     gate_whole, value_whole, down_whole = (
         lax.all_gather(gate_weight, "sp", axis=0, tiled=True),
-        lax.all_gather(value_weight, "sp", axis=0, tiled=True),
+        jnp.concatenate(
+            lax.all_to_all(jnp.stack([value_weight] * lax.axis_size("sp")), "sp", 0, 0), axis=0
+        ),
         lax.all_gather(down_weight, "sp", axis=0, tiled=True),
     )
     attended = attend(queries, keys_values, sink_logits, doc_ids, offset)

time: 374 us -> 380 us (1.016)
  waiting for transfers between devices: 268 us -> 258 us
  starting transfers between devices: 11.1 us -> 18.7 us
  local copies, waits for them, and re-layouts: 22.1 us -> 29.5 us
    all_gather x1, waiting for transfers between devices: 0.01 us -> 87.7 us  [on_device(): lax.all_gather(gate_weight, 'sp', axis=0, tiled=True)]
    all_gather x1 -> x0, waiting for transfers between devices: 47.1 us -> none  [on_device(): lax.all_gather(value_weight, 'sp', axis=0, tiled=True)]
    all_gather x1, waiting for transfers between devices: 86 us -> 45.2 us  [on_device(): lax.all_gather(down_weight, 'sp', axis=0, tiled=True)]
    psum x1, waiting for transfers between devices: 86.5 us -> 76.8 us  [on_device(): lax.psum(partial_value.astype(jnp.bfloat16), 'tp').astype(jnp.float32)]
    all_to_all x0 -> x1, starting transfers between devices: none -> 7.66 us  [on_device(): lax.all_to_all(jnp.stack([value_weight] * lax.axis_size('sp')), 'sp', 0, 0)]
  transfers between devices with their start and end apart: 9 -> 9, of which waited for: 5 -> 5; matrix products, arithmetic and copies ran while one was open for 11% -> 12% of each run, Pallas kernels for 0% -> 0%
where the time goes in v1:
time: 380 us; the launch traced here: 379 us
  waiting for transfers between devices  258 us (68%)
  matrix products  39.5 us (10%)
  local copies, waits for them, and re-layouts  29.5 us (8%)
  starting transfers between devices  18.7 us (5%)
  other arithmetic  18.4 us (5%)
  between operations  15.1 us (4%)
    all_gather x1, waiting for transfers between devices, on_device(): lax.all_gather(gate_weight, 'sp', axis=0, tiled=True)  87.7 us
    psum x1, waiting for transfers between devices, on_device(): lax.psum(partial_value.astype(jnp.bfloat16), 'tp').astype(jnp.float32)  76.8 us
    all_gather x1, waiting for transfers between devices, on_device(): lax.all_gather(down_weight, 'sp', axis=0, tiled=True)  45.2 us
    reduce_scatter x1, waiting for transfers between devices, on_device(): lax.psum_scatter(lax.dot_general(hidden, down_whole, contract_last, prefe...  43 us
    dot_general x1, matrix products, on_device(): lax.dot_general(hidden, down_whole, contract_last, preferred_element_type...  22.8 us
    concatenate x1, local copies, waits for them, and re-layouts, extended_2(): jnp.concatenate([lax.ppermute(tail, axis, [(i, (i + 1) % count) for i in...  16.7 us
    dot_general x1, matrix products, on_device(): gate_pre = jnp.dot(normed, gate_whole, preferred_element_type=jnp.float32)  9.2 us
    ppermute x2, starting transfers between devices, extended_2(): lax.ppermute(tail, axis, [(i, (i + 1) % count) for i in range(ends)])  8.12 us
  transfers between devices with their start and end apart: 9, of which 5 were waited for; matrix products, arithmetic and copies ran while one was open for 12% of the time, Pallas kernels for 0%

profile of v1, /device:TPU:0, one launch (start us, length us, event | category | flops | bytes accessed | tf_op | source)
XLA Modules:
  0.0 379.1 jit_solution(8039133650471578305)
XLA Ops:
  8.6 4.9 %collective-permute-start = (bf16[128,2,128]{2,0,1:T(8,128)(2,1)S(1)}, bf16[128,2,128]{2,0,1:T(8,128)(2,1)S(1)}, u32[]{:S(2)}, u32[]{:S(2)}) collective-permute-start(bf16[128,2,128]{2,0,1:T(8,128)(2,1)S(1)} %get-tuple-element.14), channel_id=1, source_target_pairs={{0,4},{4,8},{8,12},{12,16},{16,20},{20,24},{24,28},{1,5},{5,9},{9,... | collective-permute-start | bytes 196616 | tf_op jit(solution)/shard_map/ppermute | solution.py:21
  13.5 1.3 collective-permute-start.1
  16.4 1.3 copy.20
  17.7 3.7 reshape.106
  23.9 2.5 fusion.17
  26.4 1.5 fusion.3
  28.0 1.8 fusion.20
  30.2 3.3 convolution_convert_fusion.2
  34.0 2.6 stack.2
  36.6 7.7 %all-to-all-start = ((bf16[8,256,1280]{2,1,0:T(8,128)(2,1)}), bf16[8,256,1280]{2,1,0:T(8,128)(2,1)}, u32[]{:S(2)}, u32[]{:S(2)}) async-start(bf16[8,256,1280]{2,1,0:T(8,128)(2,1)} %stack.2), calls=%async_computation | async-start | bytes 10485760 | tf_op jit(solution)/shard_map/all_to_all | solution.py:95
  45.2 76.8 %all-reduce.4.cloned.1.call-done = bf16[1024,2048]{1,0:T(8,128)(2,1)} async-done(((bf16[1024,2048]{1,0:T(8,128)(2,1)}), bf16[1024,2048]{1,0:T(8,128)(2,1)}) %all-reduce.4.cloned.1.call-update) | async-done | bytes 4194320 | tf_op jit(solution)/shard_map/psum | solution.py:101
  122.0 7.4 %fusion = (f32[1024]{0:T(1024)S(1)}, bf16[1024,2048]{1,0:T(8,128)(2,1)}) fusion(bf16[1024,2048]{1,0:T(8,128)(2,1)} %all-reduce.4.cloned.1.call-done, bf16[1024,2048]{1,0:T(8,128)(2,1)} %param.15), kind=kLoop, calls=%fused_computation.2 | loop fusion | flops 14679040 | bytes 12587008 | tf_op jit(solution)/shard_map/reduce_sum | solution.py:37
  129.4 87.7 %all-gather.3.cloned.1.call-done = bf16[2048,1280]{1,0:T(8,128)(2,1)} async-done(((bf16[256,1280]{1,0:T(8,128)(2,1)}), bf16[2048,1280]{1,0:T(8,128)(2,1)}) %all-gather.3.cloned.1.call-update) | async-done | bytes 5242896 | tf_op jit(solution)/shard_map/all_gather | solution.py:93
  217.1 9.2 %convolution_convert_fusion = bf16[1024,1280]{1,0:T(8,128)(2,1)S(1)} fusion(bf16[2048,1280]{1,0:T(8,128)(2,1)} %all-gather.3.cloned.1.call-done, bf16[1024,2048]{1,0:T(8,128)(2,1)} %get-tuple-element.9, f32[2048]{0:T(1024)S(1)} %copy-done.8, f32[1024]{0:T(1024)S(1)} %add_rsqrt_fusion), kind=kOutput, calls=%fused_computation.28 | convolution fusion | flops 5378408448 | bytes 12070912 | tf_op jit(solution)/shard_map/dot_general | solution.py:105
  226.4 1.5 copy-done.2
  227.9 3.2 collective-permute-start.2
  231.1 1.3 collective-permute-start.3
  232.5 4.1 %collective-permute-done.3 = bf16[1,1280]{1,0:T(2,128)(2,1)S(1)} collective-permute-done((bf16[1,1280]{1,0:T(2,128)(2,1)S(1)}, bf16[1,1280]{1,0:T(2,128)(2,1)S(1)}, u32[]{:S(2)}, u32[]{:S(2)}) %collective-permute-start.3) | collective-permute-done | bytes 2592 | tf_op jit(solution)/shard_map/ppermute | solution.py:23
  236.6 16.7 %concatenate.20 = bf16[1026,1280]{1,0:T(8,128)(2,1)} concatenate(bf16[1,1280]{1,0:T(2,128)(2,1)S(1)} %collective-permute-done.2, bf16[1024,1280]{1,0:T(8,128)(2,1)} %copy-done.2, bf16[1,1280]{1,0:T(2,128)(2,1)S(1)} %collective-permute-done.3), dimensions={0} | concatenate | bytes 5253120 | tf_op jit(solution)/shard_map/concatenate | solution.py:19
  253.3 4.4 %convert_element_type.69 = f32[1026,1280]{1,0:T(8,128)} convert(bf16[1026,1280]{1,0:T(8,128)(2,1)} %concatenate.20) | non-fusion elementwise | flops 1313280 | bytes 7879680 | tf_op jit(solution)/shard_map/convert_element_type | solution.py:108
  257.7 45.2 %all-gather.5.cloned.1.call-done = bf16[2048,1280]{1,0:T(8,128)(2,1)} async-done(((bf16[256,1280]{1,0:T(8,128)(2,1)}), bf16[2048,1280]{1,0:T(8,128)(2,1)}) %all-gather.5.cloned.1.call-update) | async-done | bytes 5242896 | tf_op jit(solution)/shard_map/all_gather | solution.py:97
  303.0 22.8 %convolution_convert_fusion.1 = bf16[1024,2048]{1,0:T(8,128)(2,1)} fusion(bf16[2048,1280]{1,0:T(8,128)(2,1)} %all-gather.5.cloned.1.call-done, f32[1026,1280]{1,0:T(8,128)} %convert_element_type.69, bf16[2048,1280]{1,0:T(8,128)(2,1)} %bitcast.12, f32[1024]{0:T(1024)S(1)} %get-tuple-element.17, f32[1280]{0:T(1024)S(1)} %get-tuple-element.6, ...), kind=kOutput, calls=%fused_computation.29 | convolution fusion | flops 10770186240 | bytes 34638848 | tf_op jit(solution)/shard_map/dot_general | solution.py:120
  325.8 43.0 %reduce-scatter.2.cloned.1.call-done = bf16[256,2048]{1,0:T(8,128)(2,1)} async-done(((bf16[1024,2048]{1,0:T(8,128)(2,1)}), bf16[256,2048]{1,0:T(8,128)(2,1)}) %reduce-scatter.2.cloned.1.call-update) | async-done | bytes 1048592 | tf_op jit(solution)/shard_map/reduce_scatter | solution.py:119
  368.8 2.9 add_convert_fusion.1
  (47 shorter events, 7.3 us)
Async XLA Ops:
  7.4 22.8 %copy-start = (bf16[256,2048]{1,0:T(8,128)(2,1)S(1)}, bf16[256,2048]{1,0:T(8,128)(2,1)}, u32[]{:S(2)}) copy-start(bf16[256,2048]{1,0:T(8,128)(2,1)} %param.16) | copy-start | bytes 3145732
  7.4 114.7 %all-reduce.4.cloned.1.call-start = ((), (), s32[]{:S(2)}) async-start(), calls=%async_computation.2 | async-start | bytes 8388608 | tf_op jit(solution)/shard_map/psum | solution.py:101
  8.6 12.8 %collective-permute-start = (bf16[128,2,128]{2,0,1:T(8,128)(2,1)S(1)}, bf16[128,2,128]{2,0,1:T(8,128)(2,1)S(1)}, u32[]{:S(2)}, u32[]{:S(2)}) collective-permute-start(bf16[128,2,128]{2,0,1:T(8,128)(2,1)S(1)} %get-tuple-element.14), channel_id=1, source_target_pairs={{0,4},{4,8},{8,12},{12,16},{16,20},{20,24},{24,28},{1,5},{5,9},{9,... | collective-permute-start | bytes 196616 | tf_op jit(solution)/shard_map/ppermute | solution.py:21
  13.5 8.5 %collective-permute-start.1 = (bf16[128,2,128]{2,0,1:T(8,128)(2,1)S(1)}, bf16[128,2,128]{2,0,1:T(8,128)(2,1)}, u32[]{:S(2)}, u32[]{:S(2)}) collective-permute-start(bf16[128,2,128]{2,0,1:T(8,128)(2,1)S(1)} %get-tuple-element.15), channel_id=1, source_target_pairs={{4,0},{8,4},{12,8},{16,12},{20,16},{24,20},{28,24},{5,1},{9,5},{13... | collective-permute-start | bytes 196616 | tf_op jit(solution)/shard_map/ppermute | solution.py:23
  21.4 0.6 copy-start.5
  23.6 2.8 copy-start.7
  30.2 3.9 %copy-start.3 = (bf16[256,1280]{1,0:T(8,128)(2,1)S(1)}, bf16[256,1280]{1,0:T(8,128)(2,1)}, u32[]{:S(2)}) copy-start(bf16[256,1280]{1,0:T(8,128)(2,1)} %param.19) | copy-start | bytes 1966084
  33.5 183.7 %all-gather.3.cloned.1.call-start = ((), (), s32[]{:S(2)}) async-start(), calls=%async_computation.3 | async-start | bytes 5898240 | tf_op jit(solution)/shard_map/all_gather | solution.py:93
  36.6 8.5 %copy-start.6 = (f32[3,1280]{1,0:T(4,128)S(1)}, f32[3,1280]{1,0:T(4,128)}, u32[]{:S(2)}) copy-start(f32[3,1280]{1,0:T(4,128)} %param.20) | copy-start | bytes 46084
  36.6 221.1 %all-to-all-start = ((bf16[8,256,1280]{2,1,0:T(8,128)(2,1)}), bf16[8,256,1280]{2,1,0:T(8,128)(2,1)}, u32[]{:S(2)}, u32[]{:S(2)}) async-start(bf16[8,256,1280]{2,1,0:T(8,128)(2,1)} %stack.2), calls=%async_computation | async-start | bytes 10485760 | tf_op jit(solution)/shard_map/all_to_all | solution.py:95
  44.3 258.7 %all-gather.5.cloned.1.call-start = ((), (), s32[]{:S(2)}) async-start(), calls=%async_computation.4 | async-start | bytes 5898240 | tf_op jit(solution)/shard_map/all_gather | solution.py:97
  44.9 323.9 %reduce-scatter.2.cloned.1.call-start = ((), (), s32[]{:S(2)}) async-start(), calls=%async_computation.5 | async-start | bytes 5242880 | tf_op jit(solution)/shard_map/reduce_scatter | solution.py:119
  45.2 172.0 %copy-start.8 = (f32[2048]{0:T(1024)S(1)}, f32[2048]{0:T(1024)}, u32[]{:S(2)}) copy-start(f32[2048]{0:T(1024)} %param.17) | copy-start | bytes 24580
  217.1 15.3 %copy-start.4 = (s32[8192]{0:T(1024)S(1)}, s32[8192]{0:T(1024)}, u32[]{:S(2)}) copy-start(s32[8192]{0:T(1024)} %param.14) | copy-start | bytes 98308
  226.3 1.5 copy-start.2
  227.9 4.6 %collective-permute-start.2 = (bf16[1,1280]{1,0:T(2,128)(2,1)S(1)}, bf16[1,1280]{1,0:T(2,128)(2,1)S(1)}, u32[]{:S(2)}, u32[]{:S(2)}) collective-permute-start(bf16[1,1280]{1,0:T(2,128)(2,1)S(1)} %get-tuple-element.11), channel_id=1, source_target_pairs={{0,4},{4,8},{8,12},{12,16},{16,20},{20,24},{24,28},{1,5},{5,9},{9,... | collective-permute-start | bytes 7688 | tf_op jit(solution)/shard_map/ppermute | solution.py:21
  231.1 5.5 %collective-permute-start.3 = (bf16[1,1280]{1,0:T(2,128)(2,1)S(1)}, bf16[1,1280]{1,0:T(2,128)(2,1)S(1)}, u32[]{:S(2)}, u32[]{:S(2)}) collective-permute-start(bf16[1,1280]{1,0:T(2,128)(2,1)S(1)} %get-tuple-element.10), channel_id=1, source_target_pairs={{4,0},{8,4},{12,8},{16,12},{20,16},{24,20},{28,24},{5,1},{9,5},{13... | collective-permute-start | bytes 7688 | tf_op jit(solution)/shard_map/ppermute | solution.py:23
  303.0 68.7 %copy-start.1 = (bf16[256,2048]{1,0:T(8,128)(2,1)S(1)}, bf16[256,2048]{1,0:T(8,128)(2,1)}, u32[]{:S(2)}) copy-start(bf16[256,2048]{1,0:T(8,128)(2,1)} %param.16) | copy-start | bytes 3145732
Sparse Core Ops, SparseCore 0:
  33.6 88.3 all-reduce.3
  326.0 42.7 reduce-scatter.1
Sparse Core Ops, SparseCore 1:
  36.1 180.9 all-gather.2
  219.2 83.7 all-gather.4
